TPU v7x, 32 devices: a whole 2x2x4 slice. The times are simulated.
32 devices in a mesh: sp: 8 (over z, y), tp: 4 (over x, core).
Axes of the slice: x: 2, y: 2, z: 4, core: 2. Of those that a mesh axis runs over, the one named last changes fastest.
Arguments:
- tokens: bfloat16 [4, 512, 2048], P(None, ('sp', 'tp')), may hold values from -6 to 6
- in_gain: float32 [2048], replicated, may hold values from 0.1 to 1.9
- gate_weight: bfloat16 [2048, 1024], P(None, 'tp'), may hold values from -0.125 to 0.125
- input_weight: bfloat16 [2048, 1024], P(None, 'tp'), may hold values from -0.125 to 0.125
- key_weight: bfloat16 [2048, 512], P(None, 'tp'), may hold values from -0.125 to 0.125
- query_weight: bfloat16 [2048, 512], P(None, 'tp'), may hold values from -0.125 to 0.125
- step_weight: bfloat16 [2048, 16], replicated, may hold values from -0.125 to 0.125
- conv_input: float32 [4, 1024], P(None, 'tp'), may hold values from -3 to 3
- conv_key: float32 [4, 512], P(None, 'tp'), may hold values from -3 to 3
- conv_query: float32 [4, 512], P(None, 'tp'), may hold values from -3 to 3
- step_bias: float32 [16], P('tp'), may hold values from -5 to 1
- decay_rate: float32 [16], P('tp'), may hold values from 0 to 1, as said below
- decay_extra: float32 [4, 16, 512], P(None, 'tp', 'sp'), may hold values from -0.7 to 0, as said below
- out_gain: float32 [1024], P('tp'), may hold values from 0.1 to 1.9
- out_weight: bfloat16 [1024, 2048], replicated, may hold values from -0.1875 to 0.1875
Outputs:
- output: bfloat16 [4, 512, 2048], P(None, ('sp', 'tp'))
Inputs may be any that keep to these rules, and one draw needn't show every extreme that they name: `decay_rate`: one positive rate a head. `decay_extra`: never positive.
All inputs are finite; a program needn't handle non-finite values.
Results may differ from a plain program's by a relative error of at most 0.0072.
Values may be sent and summed in bfloat16 or wider, within the bound.
A program may use at most 128 MiB of HBM per device.

v0:
```python
import jax
import jax.numpy as jnp
from jax import lax
from jax.sharding import PartitionSpec as P

HEAD_TOTAL = 16
HEAD_DIM = 64
GROUPS = 8
STATE = 64
CONV = 4
BLOCK = 64


NORM_EPS = 1e-06
PRECISE = lax.Precision.HIGHEST


def from_behind(array, axis, by):
    length = lax.axis_size(axis)
    pairs = [(i, i + by) for i in range(length) if 0 <= i + by < length]
    return lax.ppermute(array, axis, pairs)


def carried_in(array, axis, combine, identity):
    length, place = (lax.axis_size(axis), lax.axis_index(axis))
    everything = jax.tree.map(lambda part: lax.all_gather(part, axis), array)
    start = jax.tree.map(
        lambda part, zero: jnp.broadcast_to(jnp.asarray(zero, part.dtype), part.shape),
        array,
        identity,
    )

    def step(k, before):
        reached = k < place
        new = combine(before, jax.tree.map(lambda part: part[k], everything))
        return jax.tree.map(lambda a, b: jnp.where(reached, a, b), new, before)

    return lax.fori_loop(0, length, step, start)


def rms_rows(values, gain_row):
    mean_sq = jnp.mean(values * values, axis=-1, keepdims=True)
    return values * lax.rsqrt(mean_sq + NORM_EPS) * gain_row


def causal_blend(rim_rows, local_rows, weights):
    length = local_rows.shape[1]
    padded = jnp.concatenate([rim_rows, local_rows], axis=1).astype(jnp.float32)
    summed_rows = padded[:, 0:length, :] * weights[0]
    for offset in range(1, weights.shape[0]):
        summed_rows = summed_rows + padded[:, offset : offset + length, :] * weights[offset]
    return jax.nn.silu(summed_rows)


def local_pass(scaled_x, keys_b, readout_vectors, log_decay):
    seq_count, seg_len, heads_here = (scaled_x.shape[0], scaled_x.shape[1], scaled_x.shape[2])
    blocks_here = seg_len // BLOCK
    ratio_heads = HEAD_TOTAL // GROUPS

    def to_blocks(tensor):
        return tensor.reshape((seq_count, blocks_here, BLOCK) + tensor.shape[2:])

    x_blocks = to_blocks(scaled_x)
    b_blocks = to_blocks(keys_b)
    c_blocks = to_blocks(readout_vectors)
    inside_block = jnp.cumsum(to_blocks(log_decay), axis=2)
    causal = jnp.tril(jnp.ones((BLOCK, BLOCK), bool))[None, None, :, :, None]
    spread_log = inside_block[:, :, :, None, :] - inside_block[:, :, None, :, :]
    decay_matrix = jnp.where(causal, jnp.exp(jnp.where(causal, spread_log, 0.0)), 0.0)
    scores = jnp.einsum("sblgn,sbtgn->sbltg", c_blocks, b_blocks, precision=PRECISE)
    scores = jnp.repeat(scores, ratio_heads, axis=4)
    key_heads = jnp.repeat(b_blocks, ratio_heads, axis=3)
    query_heads = jnp.repeat(c_blocks, ratio_heads, axis=3)
    inner_part = jnp.einsum(
        "sblth,sbthp->sblhp", scores * decay_matrix, x_blocks, precision=PRECISE
    )
    tail_weight = jnp.exp(inside_block[:, :, -1:, :] - inside_block)
    block_states = jnp.einsum(
        "sblhn,sblhp->sbhpn", key_heads, x_blocks * tail_weight[..., None], precision=PRECISE
    )
    block_totals = inside_block[:, :, -1, :]
    running = jnp.zeros((seq_count, heads_here, HEAD_DIM, STATE), jnp.float32)
    entering = [running]
    running = jnp.exp(block_totals[:, 0])[:, :, None, None] * running + block_states[:, 0]
    entering_states = jnp.stack(entering, axis=1)
    forwarded_portion = jnp.einsum(
        "sblhn,sbhpn->sblhp", query_heads, entering_states, precision=PRECISE
    )
    forwarded_portion = forwarded_portion * jnp.exp(inside_block)[..., None]
    local_out = (inner_part + forwarded_portion).reshape(seq_count, seg_len, heads_here, HEAD_DIM)
    decay_total = jnp.exp(jnp.sum(block_totals, axis=1))
    prefix_log = jnp.cumsum(log_decay, axis=1)
    return (local_out, decay_total, running, prefix_log)


def read_in(local_out, readout_vectors, prefix_log, incoming):
    query_heads = jnp.repeat(readout_vectors, HEAD_TOTAL // GROUPS, axis=2)
    carried = jnp.einsum("slhn,shpn->slhp", query_heads, incoming, precision=PRECISE)
    return local_out + carried * jnp.exp(prefix_log)[..., None]


def combine(preceding_portion, latter):
    return (
        preceding_portion[0] * latter[0],
        latter[0][:, :, None, None] * preceding_portion[1] + latter[1],
    )


def body(
    tokens,
    in_gain,
    gate_weight,
    input_weight,
    key_weight,
    query_weight,
    step_weight,
    conv_input,
    conv_key,
    conv_query,
    step_bias,
    decay_rate,
    decay_extra,
    out_gain,
    out_weight,
):
    normed = rms_rows(tokens.astype(jnp.float32), in_gain).astype(jnp.bfloat16)
    joined_weight = jnp.concatenate(
        [gate_weight, input_weight, key_weight, query_weight, step_weight], axis=1
    )
    token_segment = lax.all_gather(normed, "tp", axis=1, tiled=True)
    seq_count = token_segment.shape[0]
    row_count = token_segment.shape[1]
    result = jnp.dot(
        token_segment.reshape(seq_count * row_count, token_segment.shape[2]),
        joined_weight,
        preferred_element_type=jnp.float32,
    )
    projected = result.astype(jnp.bfloat16).reshape(seq_count, row_count, joined_weight.shape[1])
    seq_count, seg_len = (projected.shape[0], projected.shape[1])
    inner_here = gate_weight.shape[1]
    state_cols = key_weight.shape[1]
    heads_here = step_bias.shape[0]
    gate_in = projected[:, :, :inner_here]
    conv_in = projected[:, :, inner_here : 2 * inner_here + 2 * state_cols]
    step_all = projected[:, :, 2 * inner_here + 2 * state_cols :]
    rim_rows = from_behind(conv_in[:, seg_len - CONV + 1 :, :], "sp", 1)
    conv_weights = jnp.concatenate([conv_input, conv_key, conv_query], axis=1)
    conv_out = causal_blend(rim_rows, conv_in, conv_weights)
    conv_values = conv_out[:, :, :inner_here].reshape(seq_count, seg_len, heads_here, HEAD_DIM)
    keys_b = conv_out[:, :, inner_here : inner_here + state_cols].reshape(
        seq_count, seg_len, state_cols // STATE, STATE
    )
    readout_vectors = conv_out[:, :, inner_here + state_cols :].reshape(
        seq_count, seg_len, state_cols // STATE, STATE
    )
    own_steps = lax.dynamic_slice_in_dim(step_all, lax.axis_index("tp") * heads_here, heads_here, 2)
    step_size = jax.nn.softplus(own_steps.astype(jnp.float32) + step_bias)
    log_decay = -step_size * decay_rate + jnp.transpose(decay_extra, (0, 2, 1))
    scaled_x = conv_values * step_size[..., None]
    local_out, decay_total, final_state, prefix_log = local_pass(
        scaled_x, keys_b, readout_vectors, log_decay
    )
    incoming = carried_in(
        (decay_total, final_state),
        "sp",
        combine,
        (jnp.ones_like(decay_total), jnp.zeros_like(final_state)),
    )
    blended_heads = read_in(local_out, readout_vectors, prefix_log, incoming[1])
    gated_rows = blended_heads.reshape(seq_count, seg_len, inner_here) * jax.nn.silu(
        gate_in.astype(jnp.float32)
    )
    group_width = HEAD_TOTAL // GROUPS * HEAD_DIM
    groups_here = inner_here // group_width
    normed_out = rms_rows(
        gated_rows.reshape(seq_count, seg_len, groups_here, group_width),
        out_gain.reshape(groups_here, group_width),
    )
    normed_out = normed_out.reshape(seq_count, seg_len, inner_here).astype(jnp.bfloat16)
    token_rows = lax.all_to_all(normed_out, "tp", split_axis=1, concat_axis=2, tiled=True)
    result = jnp.dot(
        token_rows.reshape(token_rows.shape[0] * token_rows.shape[1], token_rows.shape[2]),
        out_weight,
        preferred_element_type=jnp.float32,
    )
    return result.astype(jnp.bfloat16).reshape(
        token_rows.shape[0], token_rows.shape[1], out_weight.shape[1]
    )


def solution(mesh):
    placed = (
        P(None, ("sp", "tp"), None),
        P(),
        P(None, "tp"),
        P(None, "tp"),
        P(None, "tp"),
        P(None, "tp"),
        P(),
        P(None, "tp"),
        P(None, "tp"),
        P(None, "tp"),
        P("tp"),
        P("tp"),
        P(None, "tp", "sp"),
        P("tp"),
        P(),
    )
    return jax.shard_map(
        body, mesh=mesh, in_specs=placed, out_specs=P(None, ("sp", "tp"), None), check_vma=False
    )
```

profile of v0, /device:TPU:0, one launch (start us, length us, event | category | flops | bytes accessed | tf_op | source)
XLA Modules:
  0.0 145.3 jit_solution(13819433519173447848)
XLA Ops:
  6.5 1.2 fusion.6
  7.8 1.8 %fusion.8 = bf16[4,16,2048]{2,1,0:T(8,128)(2,1)} fusion(bf16[4,16,2048]{2,1,0:T(8,128)(2,1)} %param.17, f32[2048]{0:T(1024)} %param.18, f32[4,16]{1,0:T(4,128)S(1)} %add_rsqrt_fusion.1), kind=kLoop, calls=%fused_computation.19 | loop fusion | flops 524288 | bytes 532736 | tf_op jit(solution)/shard_map/convert_element_type | solution.py:126
  9.7 0.7 constant_dynamic-update-slice_fusion.7
  10.3 0.7 constant_dynamic-update-slice_fusion.6
  11.0 1.1 copy.95
  12.1 0.7 constant_dynamic-update-slice_fusion.5
  12.9 2.3 %constant_dynamic-update-slice_fusion.4 = bf16[2048,784]{1,0:T(8,128)(2,1)} fusion(bf16[2048,256]{1,0:T(8,128)(2,1)} %param.19), kind=kLoop, calls=%fused_computation.60 | loop fusion | bytes 2097152
  15.2 1.1 constant_dynamic-update-slice_fusion.3
  16.3 0.9 constant_dynamic-update-slice_fusion.2
  17.2 0.9 constant_dynamic-update-slice_fusion.1
  18.1 0.9 constant_dynamic-update-slice_fusion
  19.0 10.2 %all-gather.5.cloned.1.call-done = bf16[4,64,2048]{2,1,0:T(8,128)(2,1)} async-done(((bf16[4,16,2048]{2,1,0:T(8,128)(2,1)}), bf16[4,64,2048]{2,1,0:T(8,128)(2,1)}) %all-gather.5.cloned.1.call-update) | async-done | bytes 1048592 | tf_op jit(solution)/shard_map/all_gather | solution.py:130
  29.2 3.8 %convolution_convert_fusion.1 = bf16[256,784]{0,1:T(8,128)(2,1)S(1)} fusion(bf16[256,2048]{1,0:T(8,128)(2,1)} %bitcast.98, bf16[2048,784]{1,0:T(8,128)(2,1)} %constant_dynamic-update-slice_fusion), kind=kOutput, calls=%fused_computation.4 | convolution fusion | flops 822284288 | bytes 4661248 | tf_op jit(solution)/shard_map/dot_general | solution.py:133
  34.0 3.4 %collective-permute-start = (bf16[4,3,512]{2,1,0:T(4,128)(2,1)S(1)}, bf16[4,3,512]{2,1,0:T(4,128)(2,1)S(1)}, u32[]{:S(2)}, u32[]{:S(2)}) collective-permute-start(bf16[4,3,512]{2,1,0:T(4,128)(2,1)S(1)} %slice.66), channel_id=1, source_target_pairs={{0,4},{4,8},{8,12},{12,16},{16,20},{20,24},{24,28},{1,5},{5,9},{9,... | collective-permute-start | bytes 36872 | tf_op jit(solution)/shard_map/ppermute | solution.py:21
  37.5 1.3 collective-permute-done
  39.7 1.5 %convolution_add_fusion = f32[4,4,64,64]{3,2,1,0:T(8,128)} fusion(f32[4,64,4,64]{3,1,2,0:T(8,128)S(1)} %bitcast.82, f32[4,64,4,64]{1,3,2,0:T(8,128)S(1)} %bitcast.75, f32[4,64,4]{1,2,0:T(4,128)S(1)} %copy.108, f32[4,4]{1,0:T(4,128)S(1)} %exponential_multiply_fusion, f32[4,64,4]{1,2,0:T(4,128)S(1)} %get-tuple-element.163), kind=kOutput, calls=%fused_computation.5 | convolution fusion | flops 50528256 | bytes 794688 | tf_op jit(solution)/shard_map/sblhn,sblhp->sbhpn/dot_general | solution.py:78
  41.9 28.5 %all-gather = f32[32,1,1,4]{3,2,1,0:T(1,128)S(1)} all-gather(f32[4,1,1,4]{3,2,1,0:T(1,128)S(1)} %get-tuple-element.158), channel_id=2, replica_groups=mesh['sp'=8,'tp'=4] {'sp'}, dimensions={0}, use_global_device_ids=true | all-gather | bytes 576 | tf_op jit(solution)/shard_map/all_gather | solution.py:26
  71.3 0.9 fusion.5
  72.3 1.1 fusion.4
  73.5 41.8 %all-gather.7.cloned.1.call-done = f32[32,4,64,64]{3,2,1,0:T(8,128)} async-done(((f32[4,4,64,64]{3,2,1,0:T(8,128)}), f32[32,4,64,64]{3,2,1,0:T(8,128)}) %all-gather.7.cloned.1.call-update) | async-done | bytes 2097168 | tf_op jit(solution)/shard_map/all_gather | solution.py:26
  115.2 9.7 %while.14 = (s32[]{:T(128)}, f32[4,4,64,64]{3,2,1,0:T(8,128)S(1)}, s32[]{:T(128)}, f32[8,4,4]{2,1,0:T(4,128)S(1)}, f32[8,4,4,64,64]{4,3,2,1,0:T(8,128)}, /*index=5*/s32[]{:T(128)}, s32[]{:T(128)}) while((s32[]{:T(128)}, f32[4,4,64,64]{3,2,1,0:T(8,128)S(1)}, s32[]{:T(128)}, f32[8,4,4]{2,1,0:T(4,128)S(1)}, ...), condition=%wide.region_3.4_spmd.clone, body=%wide.region_2.3_spmd.clone.sunk | while | flops 262148 | bytes 786729 | solution.py:38
  115.2 1.2 fusion.49
  116.4 1.2 fusion.49
  117.6 1.2 fusion.49
  118.8 1.2 fusion.49
  120.1 1.2 fusion.49
  121.3 1.2 fusion.49
  122.5 1.2 fusion.49
  123.7 1.2 fusion.49
  124.9 1.0 fusion.2
  127.5 7.1 %all_to_all.15 = bf16[4,64,256]{2,0,1:T(4,128)(2,1)S(1)} all-to-all(bf16[4,64,256]{2,0,1:T(4,128)(2,1)S(1)} %copy.116), channel_id=1, replica_groups=mesh['sp'=8,'tp'=4] {'tp'}, dimensions={1} | all-to-all | bytes 262144 | tf_op jit(solution)/shard_map/all_to_all | solution.py:180
  134.7 3.7 %convolution_convert_fusion = bf16[64,2048]{1,0:T(8,128)(2,1)} fusion(bf16[64,1024]{1,0:T(8,128)(2,1)S(1)} %bitcast.87, bf16[1024,2048]{1,0:T(8,128)(2,1)} %param.31), kind=kOutput, calls=%fused_computation.3 | convolution fusion | flops 268566528 | bytes 4587520 | tf_op jit(solution)/shard_map/dot_general | solution.py:181
  (75 shorter events, 5.3 us)
Async XLA Ops:
  6.5 8.6 %copy-start = (bf16[2048,256]{1,0:T(8,128)(2,1)S(1)}, bf16[2048,256]{1,0:T(8,128)(2,1)}, u32[]{:S(2)}) copy-start(bf16[2048,256]{1,0:T(8,128)(2,1)} %param.20) | copy-start | bytes 3145732
  6.5 9.7 %copy-start.1 = (bf16[2048,128]{1,0:T(8,128)(2,1)S(1)}, bf16[2048,128]{1,0:T(8,128)(2,1)}, u32[]{:S(2)}) copy-start(bf16[2048,128]{1,0:T(8,128)(2,1)} %param.21) | copy-start | bytes 1572868
  6.5 10.6 %copy-start.2 = (bf16[2048,128]{1,0:T(8,128)(2,1)S(1)}, bf16[2048,128]{1,0:T(8,128)(2,1)}, u32[]{:S(2)}) copy-start(bf16[2048,128]{1,0:T(8,128)(2,1)} %param.22) | copy-start | bytes 1572868
  6.5 22.6 %all-gather.5.cloned.1.call-start = ((), (), s32[]{:S(2)}) async-start(), calls=%async_computation.1 | async-start | bytes 1310720 | tf_op jit(solution)/shard_map/all_gather | solution.py:130
  9.6 105.6 %all-gather.7.cloned.1.call-start = ((), (), s32[]{:S(2)}) async-start(), calls=%async_computation.2 | async-start | bytes 4718592 | tf_op jit(solution)/shard_map/all_gather | solution.py:26
  19.0 14.6 %copy-start.3 = (f32[4,4,64]{2,1,0:T(4,128)S(1)}, f32[4,4,64]{2,1,0:T(4,128)}, u32[]{:S(2)}) copy-start(f32[4,4,64]{2,1,0:T(4,128)} %param.29) | copy-start | bytes 12292
  19.0 14.6 %copy-start.5 = (f32[4]{0:T(128)S(1)}, f32[4]{0:T(128)}, u32[]{:S(2)}) copy-start(f32[4]{0:T(128)} %param.27) | copy-start | bytes 52
  19.0 14.6 %copy-start.6 = (f32[4]{0:T(128)S(1)}, f32[4]{0:T(128)}, u32[]{:S(2)}) copy-start(f32[4]{0:T(128)} %param.28) | copy-start | bytes 52
  34.0 4.8 %collective-permute-start = (bf16[4,3,512]{2,1,0:T(4,128)(2,1)S(1)}, bf16[4,3,512]{2,1,0:T(4,128)(2,1)S(1)}, u32[]{:S(2)}, u32[]{:S(2)}) collective-permute-start(bf16[4,3,512]{2,1,0:T(4,128)(2,1)S(1)} %slice.66), channel_id=1, source_target_pairs={{0,4},{4,8},{8,12},{12,16},{16,20},{20,24},{24,28},{1,5},{5,9},{9,... | collective-permute-start | bytes 36872 | tf_op jit(solution)/shard_map/ppermute | solution.py:21
  124.9 2.3 %copy-start.4 = (f32[256]{0:T(256)S(1)}, f32[256]{0:T(256)}, u32[]{:S(2)}) copy-start(f32[256]{0:T(256)} %param.30) | copy-start | bytes 3076
Sparse Core Ops, SparseCore 0:
  9.7 19.4 all-gather.4
  41.4 73.7 all-gather.6
where the time goes:
time: 146 us; the launch traced here: 145 us
  waiting for transfers between devices  53.3 us (37%)
  blocking collectives  35.6 us (24%)
  other arithmetic  13.8 us (9%)
  between operations  13.8 us (9%)
  matrix products  12.7 us (9%)
  local copies, waits for them, and re-layouts  12.5 us (9%)
  starting transfers between devices  3.42 us (2%)
    all_gather x1, waiting for transfers between devices, carried_in(): everything = jax.tree.map(lambda part: lax.all_gather(part, axis), array)  41.8 us
    all_gather x1, blocking collectives, carried_in(): everything = jax.tree.map(lambda part: lax.all_gather(part, axis), array)  28.5 us
    all_gather x1, waiting for transfers between devices, body(): token_segment = lax.all_gather(normed, 'tp', axis=1, tiled=True)  10.2 us
    select_n x8, other arithmetic, step(): return jax.tree.map(lambda a, b: jnp.where(reached, a, b), new, before)  9.38 us
    unnamed x23, local copies, waits for them, and re-layouts  7.85 us
    all_to_all x1, blocking collectives, body(): lax.all_to_all(normed_out, 'tp', split_axis=1, concat_axis=2, tiled=True)  7.14 us
    dot_general x1, matrix products, body(): jnp.dot(token_segment.reshape(seq_count * row_count, token_segment.shape[...  3.84 us
    dot_general x1, matrix products, body(): jnp.dot(token_rows.reshape(token_rows.shape[0] * token_rows.shape[1], tok...  3.74 us
  transfers between devices with their start and end apart: 3, of which 3 were waited for; matrix products, arithmetic and copies ran while one was open for 9% of the time, Pallas kernels for 0%

commit v1 on v0

--- a/solution.py
+++ b/solution.py
@@ -1,6 +1,10 @@
+import functools
+
 import jax
 import jax.numpy as jnp
 from jax import lax
+from jax.experimental import pallas as pl
+from jax.experimental.pallas import tpu as pltpu
 from jax.sharding import PartitionSpec as P
 
 HEAD_TOTAL = 16
@@ -187,6 +191,346 @@
         token_rows.shape[0], token_rows.shape[1], out_weight.shape[1]
     )
 
+MESH = pl.DeviceIdType.MESH
+
+
+def fused_kernel(
+    dims,
+    tok, gain, gw, iw, kw, qw, sw, cx, ck, cq, sb, dr, de, og, ow,
+    out,
+    W, SW, OW, tokg, pay, aux, payr, auxr, mix, fin,
+    wsem, own_sem, xs, xr, ps, pr, fs, fr, ds, dsa, rs, rsa, ms, mr,
+):
+    nsp, ntp, S, R, D, inner, st, heads = dims
+    bf, f32 = jnp.bfloat16, jnp.float32
+    width = HEAD_TOTAL // GROUPS * HEAD_DIM
+    G = inner // width
+    X = ntp // 2
+    N = ntp * R
+    ratio = HEAD_TOTAL // GROUPS
+    sp = lax.axis_index("sp")
+    tp = lax.axis_index("tp")
+    x, c = tp // 2, tp % 2
+    partner = x * 2 + 1 - c
+    me = sp * ntp + tp
+    total = nsp * ntp
+
+    parts = [
+        (gw, W.at[:, 0:inner]),
+        (iw, W.at[:, inner : 2 * inner]),
+        (kw, W.at[:, 2 * inner : 2 * inner + st]),
+        (qw, W.at[:, 2 * inner + st : 2 * inner + 2 * st]),
+        (sw, SW),
+        (ow, OW),
+    ]
+    loads = [pltpu.make_async_copy(a, b, wsem.at[i]) for i, (a, b) in enumerate(parts)]
+    for load in loads[:5]:
+        load.start()
+    own = pltpu.make_async_copy(tok, tokg.at[:, tp], own_sem)
+    own.start()
+
+    barrier = pltpu.get_barrier_semaphore()
+
+    def greet(d, carry):
+        other = (me + d) % total
+        pl.semaphore_signal(
+            barrier, inc=1, device_id=(other // ntp, other % ntp), device_id_type=MESH
+        )
+        return carry
+
+    lax.fori_loop(1, total, greet, 0)
+    pl.semaphore_wait(barrier, total - 1)
+
+    def seq_of(k):
+        return (sp // G + 1 + k) % S
+
+    def cross(k, dx):
+        s = seq_of(k)
+        return pltpu.make_async_remote_copy(
+            src_ref=tok.at[s], dst_ref=tokg.at[s, tp],
+            send_sem=xs.at[dx - 1, k], recv_sem=xr.at[dx - 1, k],
+            device_id=(sp, (x + dx) % X * 2 + c), device_id_type=MESH,
+        )
+
+    def beside(k):
+        s = seq_of(k)
+        return pltpu.make_async_remote_copy(
+            src_ref=tok.at[s], dst_ref=tokg.at[s, tp],
+            send_sem=ps.at[k], recv_sem=pr.at[k],
+            device_id=(sp, partner), device_id_type=MESH,
+        )
+
+    def passed_on(k, dx):
+        s = seq_of(k)
+        source = (x - dx + X) % X * 2 + c
+        return pltpu.make_async_remote_copy(
+            src_ref=tokg.at[s, source], dst_ref=tokg.at[s, source],
+            send_sem=fs.at[dx - 1, k], recv_sem=fr.at[dx - 1, k],
+            device_id=(sp, partner), device_id_type=MESH,
+        )
+
+    for k in range(S):
+        for dx in range(1, X):
+            cross(k, dx).start()
+    for k in range(S):
+        beside(k).start()
+    loads[5].start()
+
+    def out_pair(dest):
+        args = dict(device_id=(dest, tp), device_id_type=MESH)
+        return (
+            pltpu.make_async_remote_copy(
+                src_ref=pay.at[dest], dst_ref=payr.at[sp],
+                send_sem=ds.at[dest], recv_sem=rs.at[sp], **args,
+            ),
+            pltpu.make_async_remote_copy(
+                src_ref=aux.at[dest], dst_ref=auxr.at[sp],
+                send_sem=dsa.at[dest], recv_sem=rsa.at[sp], **args,
+            ),
+        )
+
+    def project(k):
+        s = seq_of(k)
+        t = tokg[s].reshape(N, D).astype(f32)
+        scale = lax.rsqrt(jnp.mean(t * t, axis=-1, keepdims=True) + NORM_EPS)
+        n = (t * scale * gain[...]).astype(bf)
+        p = jnp.dot(n, W[...], preferred_element_type=f32)
+        steps = jnp.dot(n, SW[...], preferred_element_type=f32).astype(bf).astype(f32)
+        steps = steps.T
+        mine = steps[0:heads]
+        for j in range(1, ntp):
+            mine = jnp.where(tp == j, steps[j * heads : (j + 1) * heads], mine)
+        dt = jax.nn.softplus(mine + sb[...])
+        ld = de[s] - dt * dr[...]
+        for g in range(G):
+            dest = s * G + g
+            keys = p[:, 2 * inner + g * STATE : 2 * inner + (g + 1) * STATE]
+            queries = p[:, 2 * inner + st + g * STATE : 2 * inner + st + (g + 1) * STATE]
+            pay[dest, :, 0:width] = p[:, inner + g * width : inner + (g + 1) * width].astype(bf)
+            pay[dest, :, width : width + 2 * STATE] = jnp.concatenate(
+                [keys, queries], axis=1
+            ).astype(bf)
+            pay[dest, :, width + 2 * STATE :] = p[:, g * width : (g + 1) * width].astype(bf)
+            rows = jnp.concatenate(
+                [
+                    dt[g * ratio : (g + 1) * ratio],
+                    ld[g * ratio : (g + 1) * ratio],
+                    jnp.zeros((8 - 2 * ratio, N), f32),
+                ],
+                axis=0,
+            )
+            aux[dest] = jnp.concatenate([rows, jnp.zeros((8, 128 - N), f32)], axis=1)
+
+            @pl.when(dest != sp)
+            def _():
+                for copy in out_pair(dest):
+                    copy.start()
+
+            @pl.when(dest == sp)
+            def _():
+                pltpu.make_async_copy(pay.at[dest], payr.at[sp], rs.at[sp]).start()
+                pltpu.make_async_copy(aux.at[dest], auxr.at[sp], rsa.at[sp]).start()
+
+    for load in loads[:5]:
+        load.wait()
+    own.wait()
+    for k in range(S + 1):
+        if k < S:
+            for dx in range(1, X):
+                cross(k, dx).wait_recv()
+                passed_on(k, dx).start()
+        if k >= 1:
+            beside(k - 1).wait_recv()
+            for dx in range(1, X):
+                passed_on(k - 1, dx).wait_recv()
+            project(k - 1)
+
+    g = sp % G
+    mine_seq = sp // G
+    L = nsp * N
+
+    def pick(make):
+        chosen = make(0)
+        for j in range(1, G):
+            chosen = jnp.where(g == j, make(j), chosen)
+        return chosen
+
+    taps = pick(
+        lambda j: jnp.concatenate(
+            [
+                cx[:, j * width : (j + 1) * width],
+                ck[:, j * STATE : (j + 1) * STATE],
+                cq[:, j * STATE : (j + 1) * STATE],
+            ],
+            axis=1,
+        )
+    )
+    gain_out = pick(lambda j: og[:, j * width : (j + 1) * width])
+
+    for b in range(nsp):
+        pltpu.make_async_copy(payr.at[b], payr.at[b], rs.at[b]).wait()
+        pltpu.make_async_copy(auxr.at[b], auxr.at[b], rsa.at[b]).wait()
+
+    A = auxr[...].reshape(nsp * 8, 128)
+    upto = lax.broadcasted_iota(jnp.int32, (128, 128), 0) <= lax.broadcasted_iota(
+        jnp.int32, (128, 128), 1
+    )
+    cum = jnp.dot(A, upto.astype(f32), precision=PRECISE, preferred_element_type=f32)
+    AT, cumT = A.T, cum.T
+    conv_w = width + 2 * STATE
+    first_head = lax.broadcasted_iota(jnp.int32, (N, width), 1) < HEAD_DIM
+    first_row = lax.broadcasted_iota(jnp.int32, (1, width), 1) < HEAD_DIM
+    causal = lax.broadcasted_iota(jnp.int32, (N, N), 0) >= lax.broadcasted_iota(
+        jnp.int32, (N, N), 1
+    )
+    row_id = lax.broadcasted_iota(jnp.int32, (N, conv_w), 0)
+    channel = tp * G + g
+
+    def result_copy(b, j):
+        return pltpu.make_async_remote_copy(
+            src_ref=mix.at[b, j],
+            dst_ref=fin.at[mine_seq, :, pl.ds(pl.multiple_of(channel * width, width), width)],
+            send_sem=ms.at[b * ntp + j], recv_sem=mr.at[me],
+            device_id=(b, j), device_id_type=MESH,
+        )
+
+    state = jnp.zeros((STATE, width), f32)
+    before = jnp.zeros((N, conv_w), f32)
+    for b in range(nsp):
+        now = payr[b, :, 0:conv_w].astype(f32)
+        acc = now * taps[CONV - 1 : CONV]
+        for k in range(1, CONV):
+            shifted = jnp.where(row_id < k, pltpu.roll(before, k, 0), pltpu.roll(now, k, 0))
+            acc = acc + shifted * taps[CONV - 1 - k : CONV - k]
+        before = now
+        v = jax.nn.silu(acc)
+        kb = v[:, width : width + STATE].astype(bf)
+        qb = v[:, width + STATE :].astype(bf)
+        r = b * 8
+        cols = [cumT[0:N, r + ratio + h : r + ratio + h + 1] for h in range(2)]
+        rows = [cum[r + ratio + h : r + ratio + h + 1, 0:N] for h in range(2)]
+        tots = [cum[r + ratio + h : r + ratio + h + 1, 127:128] for h in range(2)]
+        step = jnp.where(first_head, AT[0:N, r : r + 1], AT[0:N, r + 1 : r + 2])
+        reach = jnp.where(first_head, cols[0], cols[1])
+        total_row = jnp.where(first_row, tots[0], tots[1])
+        xd = v[:, 0:width] * step
+        xb = xd.astype(bf)
+        scores = lax.dot_general(qb, kb, (((1,), (1,)), ((), ())), preferred_element_type=f32)
+        inner_parts = []
+        for h in range(2):
+            spread = jnp.where(causal, cols[h] - rows[h], 0.0)
+            weights = jnp.where(causal, scores * jnp.exp(spread), 0.0).astype(bf)
+            inner_parts.append(jnp.dot(weights, xb, preferred_element_type=f32))
+        y = jnp.where(first_head, inner_parts[0], inner_parts[1])
+        y = y + jnp.dot(qb, state.astype(bf), preferred_element_type=f32) * jnp.exp(reach)
+        tail = (xd * jnp.exp(total_row - reach)).astype(bf)
+        fresh = lax.dot_general(kb, tail, (((0,), (0,)), ((), ())), preferred_element_type=f32)
+        state = jnp.exp(total_row) * state + fresh
+        gated = y * jax.nn.silu(payr[b, :, conv_w:].astype(f32))
+        scale = lax.rsqrt(jnp.mean(gated * gated, axis=-1, keepdims=True) + NORM_EPS)
+        mix[b] = (gated * scale * gain_out).astype(bf).reshape(ntp, R, width)
+        for j in range(ntp):
+            same = jnp.logical_and(sp == b, tp == j)
+
+            @pl.when(jnp.logical_not(same))
+            def _():
+                result_copy(b, j).start()
+
+            @pl.when(same)
+            def _():
+                pltpu.make_async_copy(
+                    mix.at[b, j],
+                    fin.at[mine_seq, :, pl.ds(pl.multiple_of(channel * width, width), width)],
+                    mr.at[me],
+                ).start()
+
+    loads[5].wait()
+    for i in range(total):
+        slot = fin.at[i // ntp // G, :, pl.ds((i % ntp * G + i // ntp % G) * width, width)]
+        pltpu.make_async_copy(slot, slot, mr.at[i]).wait()
+    rows = fin[...].reshape(S * R, ntp * inner)
+    res = jnp.dot(rows, OW[...], preferred_element_type=f32)
+    out[...] = res.astype(bf).reshape(S, R, D)
+
+    for k in range(S):
+        for dx in range(1, X):
+            cross(k, dx).wait_send()
+            passed_on(k, dx).wait_send()
+        beside(k).wait_send()
+    for b in range(nsp):
+
+        @pl.when(b != sp)
+        def _():
+            for copy in out_pair(b):
+                copy.wait_send()
+
+        for j in range(ntp):
+
+            @pl.when(jnp.logical_not(jnp.logical_and(sp == b, tp == j)))
+            def _():
+                result_copy(b, j).wait_send()
+
+
+def fused_body(
+    nsp, ntp,
+    tokens, in_gain, gate_weight, input_weight, key_weight, query_weight, step_weight,
+    conv_input, conv_key, conv_query, step_bias, decay_rate, decay_extra, out_gain, out_weight,
+):
+    S, R, D = tokens.shape
+    inner, st, heads = gate_weight.shape[1], key_weight.shape[1], step_bias.shape[0]
+    dims = (nsp, ntp, S, R, D, inner, st, heads)
+    width = HEAD_TOTAL // GROUPS * HEAD_DIM
+    N, X = ntp * R, ntp // 2
+    pay_w = 2 * width + 2 * STATE
+    bf, f32 = jnp.bfloat16, jnp.float32
+    dma = pltpu.SemaphoreType.DMA
+    vmem = pl.BlockSpec(memory_space=pltpu.VMEM)
+    hbm = pl.BlockSpec(memory_space=pl.ANY)
+    return pl.pallas_call(
+        functools.partial(fused_kernel, dims),
+        out_shape=jax.ShapeDtypeStruct((S, R, out_weight.shape[1]), bf),
+        in_specs=[vmem, vmem, hbm, hbm, hbm, hbm, hbm] + [vmem] * 7 + [hbm],
+        out_specs=vmem,
+        scratch_shapes=[
+            pltpu.VMEM((D, 2 * inner + 2 * st), bf),
+            pltpu.VMEM(step_weight.shape, bf),
+            pltpu.VMEM(out_weight.shape, bf),
+            pltpu.VMEM((S, ntp, R, D), bf),
+            pltpu.VMEM((nsp, N, pay_w), bf),
+            pltpu.VMEM((nsp, 8, 128), f32),
+            pltpu.VMEM((nsp, N, pay_w), bf),
+            pltpu.VMEM((nsp, 8, 128), f32),
+            pltpu.VMEM((nsp, ntp, R, width), bf),
+            pltpu.VMEM((S, R, ntp * inner), bf),
+            dma((6,)),
+            dma,
+            dma((X - 1, S)), dma((X - 1, S)),
+            dma((S,)), dma((S,)),
+            dma((X - 1, S)), dma((X - 1, S)),
+            dma((nsp,)), dma((nsp,)), dma((nsp,)), dma((nsp,)),
+            dma((nsp * ntp,)), dma((nsp * ntp,)),
+        ],
+        compiler_params=pltpu.CompilerParams(
+            collective_id=0, has_side_effects=True, vmem_limit_bytes=56 * 1024 * 1024
+        ),
+        name="mixer",
+    )(
+        tokens, in_gain.reshape(1, -1), gate_weight, input_weight, key_weight, query_weight,
+        step_weight, conv_input, conv_key, conv_query, step_bias.reshape(-1, 1),
+        decay_rate.reshape(-1, 1), decay_extra, out_gain.reshape(1, -1), out_weight,
+    )
+
+
+def fits(nsp, ntp, tokens, inner, st, length):
+    seqs = tokens[0]
+    width = HEAD_TOTAL // GROUPS * HEAD_DIM
+    rows = length // (nsp * ntp)
+    return (
+        ntp % 2 == 0 and ntp > 2 and inner % width == 0 and width == 128
+        and 2 * STATE == 128 and HEAD_TOTAL // GROUPS == 2
+        and seqs * (inner // width) == nsp and rows % 16 == 0 and rows * ntp == BLOCK
+    )
+
 
 def solution(mesh):
     placed = (
@@ -206,6 +550,15 @@
         P("tp"),
         P(),
     )
+    nsp, ntp = mesh.shape["sp"], mesh.shape["tp"]
+
+    def chosen(*args):
+        inner, st = args[2].shape[1], args[4].shape[1]
+        rows = args[0].shape[1] * nsp * ntp
+        if fits(nsp, ntp, args[0].shape, inner, st, rows):
+            return fused_body(nsp, ntp, *args)
+        return body(*args)
+
     return jax.shard_map(
-        body, mesh=mesh, in_specs=placed, out_specs=P(None, ("sp", "tp"), None), check_vma=False
-    )
+        chosen, mesh=mesh, in_specs=placed, out_specs=P(None, ("sp", "tp"), None), check_vma=False
+    )

time: 146 us -> 40 us (0.27)
  waiting for transfers between devices: 53.3 us -> 0 us
  blocking collectives: 35.6 us -> 0 us
  Pallas kernels: 0 us -> 33.6 us
  other arithmetic: 13.8 us -> 0 us
  between operations: 13.8 us -> 0.01 us
  matrix products: 12.7 us -> 0 us
  local copies, waits for them, and re-layouts: 12.5 us -> 6.14 us
  starting transfers between devices: 3.42 us -> 0 us
    all_gather x2 -> x0, waiting for transfers between devices: 52 us -> none  [the longest x1 41.8 us: carried_in(): everything = jax.tree.map(lambda part: lax.all_gather(part, axis), array)]
    pallas_call x0 -> x1, Pallas kernels: none -> 33.6 us  [fused_body(): pl.pallas_call(functools.partial(fused_kernel, dims), out_shape=jax.Shape...]
    all_gather x1 -> x0, blocking collectives: 28.5 us -> none  [carried_in(): everything = jax.tree.map(lambda part: lax.all_gather(part, axis), array)]
    dot_general x7 -> x0, matrix products: 12.7 us -> none  [the longest x1 3.84 us: body(): jnp.dot(token_segment.reshape(seq_count * row_count, token_segment.shape[...]
    select_n x9 -> x0, other arithmetic: 9.47 us -> none  [the longest x8 9.38 us: step(): return jax.tree.map(lambda a, b: jnp.where(reached, a, b), new, before)]
    all_to_all x1 -> x0, blocking collectives: 7.14 us -> none  [body(): lax.all_to_all(normed_out, 'tp', split_axis=1, concat_axis=2, tiled=True)]
    unnamed x23 -> x2, local copies, waits for them, and re-layouts: 7.85 us -> 3.51 us
    ppermute x1 -> x0, starting transfers between devices: 3.38 us -> none  [from_behind(): return lax.ppermute(array, axis, pairs)]
  transfers between devices with their start and end apart: 3 -> 0, of which waited for: 3 -> 0; matrix products, arithmetic and copies ran while one was open for 9% -> 0% of each run, Pallas kernels for 0% -> 0%
where the time goes in v1:
time: 40 us; the launch traced here: 39.8 us
  Pallas kernels  33.6 us (84%)
  local copies, waits for them, and re-layouts  6.14 us (15%)
    pallas_call x1, Pallas kernels, fused_body(): pl.pallas_call(functools.partial(fused_kernel, dims), out_shape=jax.Shape...  33.6 us
    unnamed x2, local copies, waits for them, and re-layouts  3.51 us
    reshape x1, local copies, waits for them, and re-layouts, fused_body(): decay_rate.reshape(-1, 1)  1.32 us
    reshape x1, local copies, waits for them, and re-layouts, fused_body(): step_bias.reshape(-1, 1)  1.31 us

profile of v1, /device:TPU:0, one launch (start us, length us, event | category | flops | bytes accessed | tf_op | source)
XLA Modules:
  0.0 39.8 jit_solution(16961207755171126792)
XLA Ops:
  0.0 1.3 %copy.17.sb = f32[4,1]{1,0:T(4,128)} copy(f32[4,1]{0,1:T(1,128)} %bitcast.6) | data formatting | bytes 32 | tf_op jit(solution)/shard_map/reshape | solution.py:519
  1.3 1.3 %copy.18.dr = f32[4,1]{1,0:T(4,128)} copy(f32[4,1]{0,1:T(1,128)} %bitcast.7) | data formatting | bytes 32 | tf_op jit(solution)/shard_map/reshape | solution.py:520
  2.6 1.8 %copy.16.sw = bf16[2048,16]{1,0:T(8,128)(2,1)} copy(bf16[2048,16]{0,1:T(8,128)(2,1)} %param.21) | data formatting | bytes 131072 | tf_op args[6]
  4.5 33.6 %mixer.1 = bf16[4,16,2048]{2,1,0:T(8,128)(2,1)} custom-call(bf16[4,16,2048]{2,1,0:T(8,128)(2,1)} %tok.1, f32[1,2048]{1,0:T(1,128)} %bitcast.4, bf16[2048,256]{1,0:T(8,128)(2,1)} %gw.1, bf16[2048,256]{1,0:T(8,128)(2,1)} %iw.1, bf16[2048,128]{1,0:T(8,128)(2,1)} %kw.1, bf16[2048,128]{1,0:T(8,128)(2,1)} %qw.1, bf16[2048,16]{1,0:T(8,128)(2,1)} %copy.16.sw, ...), custom_call_target="tpu_custom_call" | custom-call | tf_op jit(solution)/shard_map/mixer/pallas_call | solution.py:489
  38.1 1.7 %copy.20 = bf16[4,16,2048]{2,1,0:T(8,128)(2,1)} copy(bf16[4,16,2048]{2,1,0:T(8,128)(2,1)} %mixer.1) | data formatting | bytes 524288

commit v2 on v1

--- a/solution.py
+++ b/solution.py
@@ -199,7 +199,7 @@
     tok, gain, gw, iw, kw, qw, sw, cx, ck, cq, sb, dr, de, og, ow,
     out,
     W, SW, OW, tokg, pay, aux, payr, auxr, mix, fin,
-    wsem, own_sem, xs, xr, ps, pr, fs, fr, ds, dsa, rs, rsa, ms, mr,
+    wsem, own_sem, xs, xr, ps, pr, fs, fr, ds, dsa, rs, rsa, ms, mr, round_sem,
 ):
     nsp, ntp, S, R, D, inner, st, heads = dims
     bf, f32 = jnp.bfloat16, jnp.float32
@@ -231,15 +231,31 @@
 
     barrier = pltpu.get_barrier_semaphore()
 
-    def greet(d, carry):
-        other = (me + d) % total
+    def near(sem):
+        row = sp // G
+        for d in range(1, G):
+            other = row * G + (sp + d) % G
+            pl.semaphore_signal(sem, inc=1, device_id=(other, tp), device_id_type=MESH)
+
+        @pl.when(row > 0)
+        def _():
+            pl.semaphore_signal(sem, inc=1, device_id=(sp - G, tp), device_id_type=MESH)
+
+        @pl.when(row < S - 1)
+        def _():
+            pl.semaphore_signal(sem, inc=1, device_id=(sp + G, tp), device_id_type=MESH)
+
+    def near_wait(sem, extra):
+        row = sp // G
+        ends = jnp.where(row > 0, 1, 0) + jnp.where(row < S - 1, 1, 0)
+        pl.semaphore_wait(sem, G - 1 + extra + ends)
+
+    for d in range(1, ntp):
         pl.semaphore_signal(
-            barrier, inc=1, device_id=(other // ntp, other % ntp), device_id_type=MESH
-        )
-        return carry
-
-    lax.fori_loop(1, total, greet, 0)
-    pl.semaphore_wait(barrier, total - 1)
+            barrier, inc=1, device_id=(sp, (tp + d) % ntp), device_id_type=MESH
+        )
+    near(barrier)
+    near_wait(barrier, ntp - 1)
 
     def seq_of(k):
         return (sp // G + 1 + k) % S
@@ -275,6 +291,9 @@
     for k in range(S):
         beside(k).start()
     loads[5].start()
+    for i in range(S - 1):
+        near(round_sem.at[i])
+        near_wait(round_sem.at[i], 0)
 
     def out_pair(dest):
         args = dict(device_id=(dest, tp), device_id_type=MESH)
@@ -289,19 +308,28 @@
             ),
         )
 
+    head_id = lax.broadcasted_iota(jnp.int32, (heads, N), 0)
+    bias_col = jnp.zeros((heads, N), f32)
+    rate_col = jnp.zeros((heads, N), f32)
+    for h in range(heads):
+        bias_col = jnp.where(head_id == h, sb[h], bias_col)
+        rate_col = jnp.where(head_id == h, dr[h], rate_col)
+
     def project(k):
         s = seq_of(k)
         t = tokg[s].reshape(N, D).astype(f32)
         scale = lax.rsqrt(jnp.mean(t * t, axis=-1, keepdims=True) + NORM_EPS)
         n = (t * scale * gain[...]).astype(bf)
         p = jnp.dot(n, W[...], preferred_element_type=f32)
-        steps = jnp.dot(n, SW[...], preferred_element_type=f32).astype(bf).astype(f32)
-        steps = steps.T
+        steps = lax.dot_general(
+            SW[...], n, (((1,), (1,)), ((), ())), preferred_element_type=f32
+        )
+        steps = steps.astype(bf).astype(f32)
         mine = steps[0:heads]
         for j in range(1, ntp):
             mine = jnp.where(tp == j, steps[j * heads : (j + 1) * heads], mine)
-        dt = jax.nn.softplus(mine + sb[...])
-        ld = de[s] - dt * dr[...]
+        dt = jax.nn.softplus(mine + bias_col)
+        ld = de[s] - dt * rate_col
         for g in range(G):
             dest = s * G + g
             keys = p[:, 2 * inner + g * STATE : 2 * inner + (g + 1) * STATE]
@@ -486,14 +514,15 @@
     dma = pltpu.SemaphoreType.DMA
     vmem = pl.BlockSpec(memory_space=pltpu.VMEM)
     hbm = pl.BlockSpec(memory_space=pl.ANY)
+    smem = pl.BlockSpec(memory_space=pltpu.SMEM)
     return pl.pallas_call(
         functools.partial(fused_kernel, dims),
         out_shape=jax.ShapeDtypeStruct((S, R, out_weight.shape[1]), bf),
-        in_specs=[vmem, vmem, hbm, hbm, hbm, hbm, hbm] + [vmem] * 7 + [hbm],
+        in_specs=[vmem, vmem, hbm, hbm, hbm, hbm, hbm] + [vmem] * 3 + [smem] * 2 + [vmem] * 2 + [hbm],
         out_specs=vmem,
         scratch_shapes=[
             pltpu.VMEM((D, 2 * inner + 2 * st), bf),
-            pltpu.VMEM(step_weight.shape, bf),
+            pltpu.VMEM(step_weight.shape[::-1], bf),
             pltpu.VMEM(out_weight.shape, bf),
             pltpu.VMEM((S, ntp, R, D), bf),
             pltpu.VMEM((nsp, N, pay_w), bf),
@@ -509,6 +538,7 @@
             dma((X - 1, S)), dma((X - 1, S)),
             dma((nsp,)), dma((nsp,)), dma((nsp,)), dma((nsp,)),
             dma((nsp * ntp,)), dma((nsp * ntp,)),
+            pltpu.SemaphoreType.REGULAR((S - 1,)),
         ],
         compiler_params=pltpu.CompilerParams(
             collective_id=0, has_side_effects=True, vmem_limit_bytes=56 * 1024 * 1024
@@ -516,8 +546,7 @@
         name="mixer",
     )(
         tokens, in_gain.reshape(1, -1), gate_weight, input_weight, key_weight, query_weight,
-        step_weight, conv_input, conv_key, conv_query, step_bias.reshape(-1, 1),
-        decay_rate.reshape(-1, 1), decay_extra, out_gain.reshape(1, -1), out_weight,
+        step_weight.T, conv_input, conv_key, conv_query, step_bias, decay_rate, decay_extra, out_gain.reshape(1, -1), out_weight,
     )
 
 

time: 40 us -> 33.1 us (0.83)
  local copies, waits for them, and re-layouts: 6.14 us -> 1.67 us
  Pallas kernels: 33.6 us -> 31 us
    reshape x2 -> x0, local copies, waits for them, and re-layouts: 2.63 us -> none  [the longest x1 1.32 us: fused_body(): decay_rate.reshape(-1, 1)]
    pallas_call x1, Pallas kernels: 33.6 us -> 31 us  [fused_body(): pl.pallas_call(functools.partial(fused_kernel, dims), out_shape=jax.Shape...]
    unnamed x2 -> x1, local copies, waits for them, and re-layouts: 3.51 us -> 1.67 us
where the time goes in v2:
time: 33.1 us; the launch traced here: 32.7 us
  Pallas kernels  31 us (94%)
  local copies, waits for them, and re-layouts  1.67 us (5%)
    pallas_call x1, Pallas kernels, fused_body(): pl.pallas_call(functools.partial(fused_kernel, dims), out_shape=jax.Shape...  31 us
    unnamed x1, local copies, waits for them, and re-layouts  1.67 us

profile of v2, /device:TPU:0, one launch (start us, length us, event | category | flops | bytes accessed | tf_op | source)
XLA Modules:
  0.0 32.7 jit_solution(5594076265765807309)
XLA Ops:
  0.0 31.0 %mixer.1 = bf16[4,16,2048]{2,1,0:T(8,128)(2,1)} custom-call(bf16[4,16,2048]{2,1,0:T(8,128)(2,1)} %tok.1, f32[1,2048]{1,0:T(1,128)} %bitcast.4, bf16[2048,256]{1,0:T(8,128)(2,1)} %gw.1, bf16[2048,256]{1,0:T(8,128)(2,1)} %iw.1, bf16[2048,128]{1,0:T(8,128)(2,1)} %kw.1, bf16[2048,128]{1,0:T(8,128)(2,1)} %qw.1, bf16[16,2048]{1,0:T(8,128)(2,1)} %bitcast.3, ...), custom_call_target="tpu_custom_call" | custom-call | tf_op jit(solution)/shard_map/mixer/pallas_call | solution.py:518
  31.0 1.7 %copy.17 = bf16[4,16,2048]{2,1,0:T(8,128)(2,1)} copy(bf16[4,16,2048]{2,1,0:T(8,128)(2,1)} %mixer.1) | data formatting | bytes 524288

commit v3 on v2

--- a/solution.py
+++ b/solution.py
@@ -396,7 +396,6 @@
     gain_out = pick(lambda j: og[:, j * width : (j + 1) * width])
 
     for b in range(nsp):
-        pltpu.make_async_copy(payr.at[b], payr.at[b], rs.at[b]).wait()
         pltpu.make_async_copy(auxr.at[b], auxr.at[b], rsa.at[b]).wait()
 
     A = auxr[...].reshape(nsp * 8, 128)
@@ -425,6 +424,7 @@
     state = jnp.zeros((STATE, width), f32)
     before = jnp.zeros((N, conv_w), f32)
     for b in range(nsp):
+        pltpu.make_async_copy(payr.at[b], payr.at[b], rs.at[b]).wait()
         now = payr[b, :, 0:conv_w].astype(f32)
         acc = now * taps[CONV - 1 : CONV]
         for k in range(1, CONV):

time: 33.1 us -> 33.2 us (level)
  no operation moved by 1% of the time
where the time goes in v3:
time: 33.2 us; the launch traced here: 32.8 us
  Pallas kernels  31.1 us (94%)
  local copies, waits for them, and re-layouts  1.67 us (5%)
    pallas_call x1, Pallas kernels, fused_body(): pl.pallas_call(functools.partial(fused_kernel, dims), out_shape=jax.Shape...  31.1 us
    unnamed x1, local copies, waits for them, and re-layouts  1.67 us

profile of v3, /device:TPU:0, one launch (start us, length us, event | category | flops | bytes accessed | tf_op | source)
XLA Modules:
  0.0 32.8 jit_solution(8763323302844035788)
XLA Ops:
  0.0 31.1 %mixer.1 = bf16[4,16,2048]{2,1,0:T(8,128)(2,1)} custom-call(bf16[4,16,2048]{2,1,0:T(8,128)(2,1)} %tok.1, f32[1,2048]{1,0:T(1,128)} %bitcast.4, bf16[2048,256]{1,0:T(8,128)(2,1)} %gw.1, bf16[2048,256]{1,0:T(8,128)(2,1)} %iw.1, bf16[2048,128]{1,0:T(8,128)(2,1)} %kw.1, bf16[2048,128]{1,0:T(8,128)(2,1)} %qw.1, bf16[16,2048]{1,0:T(8,128)(2,1)} %bitcast.3, ...), custom_call_target="tpu_custom_call" | custom-call | tf_op jit(solution)/shard_map/mixer/pallas_call | solution.py:518
  31.1 1.7 %copy.17 = bf16[4,16,2048]{2,1,0:T(8,128)(2,1)} copy(bf16[4,16,2048]{2,1,0:T(8,128)(2,1)} %mixer.1) | data formatting | bytes 524288
